TPU v7x, 256 devices: a whole 4x4x8 slice. The times are simulated.
256 devices in a mesh: ep: 64 (over z, x, core), tp: 4 (over y).
Axes of the slice: x: 4, y: 4, z: 8, core: 2. Of those that a mesh axis runs over, the one named last changes fastest.
Arguments:
- gate_branch: bfloat16 [32768, 2048], P(('ep', 'tp')), may hold values from -8 to 8
- rec_branch: bfloat16 [32768, 2048], P(('ep', 'tp')), may hold values from -6 to 6
- conv_weight: float32 [4, 2048], replicated, may hold values from -3 to 3
- gate_a: bfloat16 [8, 256, 256], replicated, may hold values from -0.375 to 0.375
- gate_x: bfloat16 [8, 256, 256], replicated, may hold values from -0.375 to 0.375
- decay_param: float32 [2048], replicated, as said below
- decay_shift: float32 [32768], P(('ep', 'tp')), may hold values from -0.6 to 0
- tokens: bfloat16 [32768, 2048], P(('ep', 'tp')), may hold values from -6 to 6
- routes: int32 [32768, 2], P(('ep', 'tp')), may hold values from 0 to 63, all different within a row; in each aligned block of 128 rows (0 to 127, 128 to 255, ...) at most 5 rows name the same one
- route_weight: float32 [32768, 2], P(('ep', 'tp')), may hold values from 0.1 to 0.9
- norm_gain: float32 [2048], replicated, may hold values from 0.1 to 1.9
- w_gate: bfloat16 [64, 2048, 3584], P('ep', None, 'tp'), may hold values from -0.125 to 0.125
- w_up: bfloat16 [64, 2048, 3584], P('ep', None, 'tp'), may hold values from -0.125 to 0.125
- w_down: bfloat16 [64, 3584, 2048], P('ep', 'tp'), may hold values from -0.09375 to 0.09375
Outputs:
- mixed_out: bfloat16 [32768, 2048], P(('ep', 'tp'))
- expert_out: bfloat16 [32768, 2048], P(('ep', 'tp'))
Inputs may be any that keep to these rules, and one draw needn't show every extreme that they name: `routes`: in each aligned block of 128 rows (the rows of one device) no expert is named more than 5 times, and some block names some expert exactly 5 times; the experts of one row differ. 8 softplus(-decay_param) lies between 0.2 / 32768 and 0.07.
All inputs are finite; a program needn't handle non-finite values.
Results may differ from a plain program's by a relative error of at most 0.012.
Values may be sent and summed in bfloat16 or wider, within the bound.
A program may use at most 128 MiB of HBM per device.

v0:
```python
import math

import jax
import jax.numpy as jnp
from jax import lax
from jax.sharding import Mesh
from jax.sharding import PartitionSpec as P

EP_TP = ("ep_0", "ep_1", "ep_2", "tp")
EP = ("ep_0", "ep_1", "ep_2")


EPSILON = 1e-05


def passed_along(block, axis, distance):
    devices = range(lax.axis_size(axis))
    route = [(i - distance, i) for i in devices if i - distance in devices]
    return lax.ppermute(block, axis, route)


def neutral_like(array, identity):
    return jax.tree.map(
        lambda part, zero: jnp.zeros_like(part) + jnp.asarray(zero, part.dtype), array, identity
    )


def gathered_once(array, axis):
    leaves = jax.tree.leaves(array)
    sequence = sorted(range(len(leaves)), key=lambda k: -leaves[k].size)
    width = (1, *leaves[sequence[0]].shape)[-1]
    lines = [
        jnp.pad(leaves[k].reshape(-1), (0, -leaves[k].size % width)).reshape(-1, width)
        for k in sequence
    ]
    both, at, found = (lax.all_gather(jnp.concatenate(lines), axis), 0, {})
    for k, line in zip(sequence, lines):
        piece = both[:, at : at + len(line)].reshape(len(both), -1)
        found[k] = piece[:, : leaves[k].size].reshape(-1, *leaves[k].shape)
        at += len(line)
    numbers = iter(range(len(leaves)))
    return jax.tree.map(lambda _: found[next(numbers)], array)


def carried_in(array, axes, combine, identity):
    before = start = neutral_like(array, identity)
    subtotal = array
    for axis in reversed(axes):
        length, here = (lax.axis_size(axis), lax.axis_index(axis))
        pieces = gathered_once(subtotal, axis)
        inside, subtotal = (start, start)
        for k in range(length):
            passed = k < here
            subtotal = combine(subtotal, jax.tree.map(lambda part: part[k], pieces))
            inside = jax.tree.map(lambda new, old: jnp.where(passed, new, old), subtotal, inside)
        before = combine(inside, before)
    return before


def pair_combine(earlier, later):
    return (earlier[0] * later[0], later[0] * earlier[1] + later[1])


def short_conv(previous, current, conv_weight):
    tap_count = conv_weight.shape[0]
    row_count = current.shape[0]
    padded = jnp.concatenate([previous, current], 0)
    summed = jnp.zeros(current.shape, jnp.float32)
    for tap_index in range(tap_count):
        summed = summed + conv_weight[tap_index] * padded[tap_index : tap_index + row_count].astype(
            jnp.float32
        )
    return summed.astype(jnp.bfloat16)


def mixer_gates(conv_rows, gate_a, gate_x, decay_rate, shift_rows):
    row_count, width_all = conv_rows.shape
    block_count, block_width = (gate_a.shape[0], gate_a.shape[1])
    split_rows = conv_rows.reshape(row_count, block_count, block_width)
    pre_a = jnp.einsum("rnc,ncd->rnd", split_rows, gate_a, preferred_element_type=jnp.float32)
    pre_x = jnp.einsum("rnc,ncd->rnd", split_rows, gate_x, preferred_element_type=jnp.float32)
    recur_gate = jax.nn.sigmoid(pre_a.reshape(row_count, width_all))
    input_gate = jax.nn.sigmoid(pre_x.reshape(row_count, width_all))
    log_a = -decay_rate[None, :] * recur_gate + shift_rows[:, None]
    drive = jnp.sqrt(-jnp.expm1(2.0 * log_a)) * input_gate * conv_rows.astype(jnp.float32)
    return (log_a, drive)


def blocked_recurrence(decay, drive):
    row_count, width_all = decay.shape
    group = math.gcd(row_count, 8)
    block_count = row_count // group
    decay_blocks = decay.reshape(block_count, group, width_all)
    drive_blocks = drive.reshape(block_count, group, width_all)
    factors = [decay_blocks[:, 0]]
    states = [drive_blocks[:, 0]]
    for inner in range(1, group):
        factors.append(factors[-1] * decay_blocks[:, inner])
        states.append(decay_blocks[:, inner] * states[-1] + drive_blocks[:, inner])
    factor_inner = jnp.stack(factors, 1)
    state_inner = jnp.stack(states, 1)

    def carry_step(carried, totals):
        return (pair_combine(carried, totals), carried)

    start = (jnp.ones((width_all,), jnp.float32), jnp.zeros((width_all,), jnp.float32))
    _, before = lax.scan(carry_step, start, (factors[-1], states[-1]))
    factor_all = factor_inner * before[0][:, None, :]
    state_all = state_inner + factor_inner * before[1][:, None, :]
    return (factor_all.reshape(row_count, width_all), state_all.reshape(row_count, width_all))


def layer_scale(rows_in, norm_gain):
    values = rows_in.astype(jnp.float32)
    center = jnp.mean(values, -1, keepdims=True)
    spread = jnp.mean(jnp.square(values - center), -1, keepdims=True)
    return ((values - center) * lax.rsqrt(spread + EPSILON) * norm_gain).astype(jnp.bfloat16)


def slot_numbers(routes, block_rows, expert_count):
    row_count, top_count = routes.shape
    onehot = (routes[:, :, None] == jnp.arange(expert_count, dtype=jnp.int32)).astype(jnp.int32)
    ranked = (
        jnp.cumsum(
            onehot.reshape(row_count // block_rows, block_rows * top_count, expert_count), axis=1
        )
        - 1
    )
    return jnp.sum(ranked.reshape(row_count, top_count, expert_count) * onehot, -1)


def expert_hidden(rows_in, gate_part, up_part):
    return (
        jax.nn.silu(jnp.dot(rows_in, gate_part, preferred_element_type=jnp.float32))
        * jnp.dot(rows_in, up_part, preferred_element_type=jnp.float32)
    ).astype(jnp.bfloat16)


def shards(
    gate_branch,
    rec_branch,
    conv_weight,
    gate_a,
    gate_x,
    decay_param,
    decay_shift,
    tokens,
    routes,
    route_weight,
    norm_gain,
    w_gate,
    w_up,
    w_down,
):
    tap_count = conv_weight.shape[0]
    row_count, width_all = rec_branch.shape
    previous = passed_along(rec_branch[row_count - (tap_count - 1) :], EP_TP, 1)
    conv_rows = short_conv(previous, rec_branch, conv_weight)
    decay_rate = 8.0 * jax.nn.softplus(-decay_param)
    log_a, drive = mixer_gates(conv_rows, gate_a, gate_x, decay_rate, decay_shift)
    factor, local_state = blocked_recurrence(jnp.exp(log_a), drive)
    identity = (jnp.ones((width_all,), jnp.float32), jnp.zeros((width_all,), jnp.float32))
    carried = carried_in((factor[-1], local_state[-1]), EP_TP, pair_combine, identity)
    states = local_state + factor * carried[1][None, :]
    mixed_out = (states * jax.nn.gelu(gate_branch.astype(jnp.float32), approximate=True)).astype(
        jnp.bfloat16
    )
    ep_count = lax.axis_size(EP)
    block_rows, top_count = routes.shape
    capacity = max(2, block_rows * top_count * 5 // (4 * ep_count))
    normed = layer_scale(tokens, norm_gain)
    slots = slot_numbers(routes, block_rows, ep_count)
    row_ids = jnp.broadcast_to(jnp.arange(block_rows, dtype=jnp.int32)[:, None], routes.shape)
    flat = routes * capacity + slots
    table = jnp.full((ep_count * capacity,), block_rows, jnp.int32)
    table = table.at[flat.reshape(-1)].set(row_ids.reshape(-1))
    outgoing = jnp.take(normed, table, axis=0, mode="fill", fill_value=0)
    outgoing = outgoing.reshape(ep_count, capacity, width_all)
    arrived = lax.all_to_all(outgoing, EP, split_axis=0, concat_axis=0, tiled=True)
    hidden = expert_hidden(
        lax.all_gather(arrived.reshape(-1, width_all), "tp", axis=0, tiled=True), w_gate[0], w_up[0]
    )
    route_out = lax.psum_scatter(
        jnp.dot(hidden, w_down[0], preferred_element_type=jnp.float32).astype(jnp.bfloat16),
        "tp",
        scatter_dimension=0,
        tiled=True,
    )
    returned = lax.all_to_all(
        route_out.reshape(ep_count, capacity, width_all),
        EP,
        split_axis=0,
        concat_axis=0,
        tiled=True,
    )
    returned = returned.reshape(ep_count * capacity, width_all)
    picked = jnp.take(returned, flat.reshape(-1), axis=0).astype(jnp.float32)
    picked = picked.reshape(block_rows, top_count, width_all)
    expert_out = jnp.sum(picked * route_weight[:, :, None], axis=1).astype(jnp.bfloat16)
    return (mixed_out, expert_out)


def solution(mesh):
    split = Mesh(mesh.devices.reshape(8, 4, 2, mesh.shape["tp"]), ("ep_0", "ep_1", "ep_2", "tp"))
    return jax.shard_map(
        shards,
        mesh=split,
        in_specs=(
            P(EP_TP, None),
            P(EP_TP, None),
            P(),
            P(),
            P(),
            P(),
            P(EP_TP),
            P(EP_TP, None),
            P(EP_TP, None),
            P(EP_TP, None),
            P(),
            P(EP, None, "tp"),
            P(EP, None, "tp"),
            P(EP, "tp", None),
        ),
        out_specs=(P(EP_TP, None), P(EP_TP, None)),
        check_vma=False,
    )
```

profile of v0, /device:TPU:1, one launch (start us, length us, event | category | flops | bytes accessed | tf_op | source)
XLA Modules:
  0.0 313.9 jit_solution(11399140220905587292)
XLA Ops:
  7.2 0.9 copy.64
  8.3 0.6 reduce-window.6
  9.8 0.7 compare_and_fusion.1
  10.9 1.4 scatter_custom_fusion
  12.4 1.2 convert_reduce_fusion
  13.6 1.3 fusion.14
  14.9 1.4 fusion.16
  16.3 3.0 gather_fusion
  19.3 2.4 gather.13
  22.1 62.5 %all_to_all.10 = bf16[64,5,2048]{2,1,0:T(8,128)(2,1)S(1)} all-to-all(bf16[64,5,2048]{2,1,0:T(8,128)(2,1)S(1)} %broadcast_select_fusion.2), channel_id=1, replica_groups=mesh['ep_0'=8,'ep_1'=4,'ep_2'=2,'tp'=4] {'ep_0','ep_1','ep_2'}, dimensions={0} | all-to-all | bytes 2621440 | tf_op jit(solution)/shard_map/all_to_all | solution.py:179
  84.6 1.4 reshape.838
  86.1 0.8 slice.280
  87.2 3.4 %collective-permute-start = (bf16[3,2048]{0,1:T(8,128)(2,1)S(1)}, bf16[3,2048]{0,1:T(8,128)(2,1)S(1)}, u32[]{:S(2)}, u32[]{:S(2)}) collective-permute-start(bf16[3,2048]{0,1:T(8,128)(2,1)S(1)} %copy.55), channel_id=1, source_target_pairs={{0,1},{1,2},{2,3},{3,4},{4,5},{5,6},{6,7},{7,8},{8,9},{9,10},{10,1... | collective-permute-start | bytes 36872 | tf_op jit(solution)/shard_map/ppermute | solution.py:19
  90.7 0.6 pad_clamp_fusion
  91.3 1.3 copy.56
  92.8 0.7 copy.69
  93.5 0.7 copy.71
  94.2 6.8 %collective-permute-done = bf16[3,2048]{0,1:T(8,128)(2,1)S(1)} collective-permute-done((bf16[3,2048]{0,1:T(8,128)(2,1)S(1)}, bf16[3,2048]{0,1:T(8,128)(2,1)S(1)}, u32[]{:S(2)}, u32[]{:S(2)}) %collective-permute-start) | collective-permute-done | bytes 12320 | tf_op jit(solution)/shard_map/ppermute | solution.py:19
  101.0 2.1 add_convert_fusion
  103.2 0.8 copy-done.2
  103.9 0.5 fusion.11
  104.8 0.6 copy.63
  105.4 2.9 fusion.7
  108.3 1.6 copy.61
  109.8 3.0 fusion.24
  112.8 1.6 copy.62
  114.8 2.2 slice_add_fusion
  117.0 2.8 stack.4
  119.8 0.7 slice_multiply_fusion
  120.6 2.6 stack.5
  123.1 21.0 %all-gather.10.cloned.1.call-done = bf16[1280,2048]{1,0:T(8,128)(2,1)} async-done(((bf16[320,2048]{1,0:T(8,128)(2,1)}), bf16[1280,2048]{1,0:T(8,128)(2,1)}) %all-gather.10.cloned.1.call-update) | async-done | bytes 5242896 | tf_op jit(solution)/shard_map/all_gather | solution.py:181
  144.1 9.9 %fusion.2 = f32[1280,896]{1,0:T(8,128)} fusion(bf16[1280,2048]{1,0:T(8,128)(2,1)} %all-gather.10.cloned.1.call-done, bf16[1,2048,896]{2,1,0:T(8,128)(2,1)} %param.27), kind=kOutput, calls=%fused_computation.12 | convolution fusion | flops 4697620480 | bytes 13500416 | tf_op jit(solution)/shard_map/dot_general | solution.py:134
  154.0 17.6 %convolution_convert_fusion = bf16[1280,2048]{1,0:T(8,128)(2,1)} fusion(bf16[1,896,2048]{2,1,0:T(8,128)(2,1)} %param.29, f32[1280,896]{1,0:T(8,128)} %fusion.2, bf16[1280,2048]{1,0:T(8,128)(2,1)} %all-gather.10.cloned.1.call-done, bf16[1,2048,896]{2,1,0:T(8,128)(2,1)} %param.28), kind=kOutput, calls=%fused_computation.8 | convolution fusion | flops 9404743680 | bytes 22413312 | tf_op jit(solution)/shard_map/dot_general | solution.py:184
  171.7 0.8 copy-done.5
  172.6 7.8 %while.17 = (s32[]{:T(128)}, f32[2048]{0:T(1024)S(1)}, f32[2048]{0:T(1024)S(1)}, f32[16,2048]{1,0:T(8,128)S(1)}, f32[16,2048]{1,0:T(8,128)S(1)}, /*index=5*/f32[...) while((s32[]{:T(128)}, f32[2048]{0:T(1024)S(1)}, f32[2048]{0:T(1024)S(1)}, ...), condition=%wide.region_1.2_spmd.clone, body=%wide.region_0.1_spmd.clone.sunk | while | flops 10243 | bytes 131187 | solution.py:107
  180.4 1.5 multiply_bitcast_fusion
  181.9 12.6 %all-gather.4 = f32[4,2,2048]{2,1,0:T(2,128)S(1)} all-gather(f32[1,2,2048]{2,1,0:T(2,128)S(1)} %maximum_bitcast_fusion), channel_id=2, replica_groups=mesh['ep_0'=8,'ep_1'=4,'ep_2'=2,'tp'=4] {'tp'}, dimensions={0}, use_global_device_ids=true | all-gather | bytes 81920 | tf_op jit(solution)/shard_map/all_gather | solution.py:36
  194.6 3.7 %all-gather.5 = f32[2,2,2048]{2,1,0:T(2,128)S(1)} all-gather(f32[1,2,2048]{2,1,0:T(2,128)S(1)} %maximum_bitcast_fusion.1), channel_id=3, replica_groups=mesh['ep_0'=8,'ep_1'=4,'ep_2'=2,'tp'=4] {'ep_2'}, dimensions={0}, use_global_device_ids=true | all-gather | bytes 49152 | tf_op jit(solution)/shard_map/all_gather | solution.py:36
  198.4 13.5 %all-gather.6 = f32[4,2,2048]{2,1,0:T(2,128)S(1)} all-gather(f32[1,2,2048]{2,1,0:T(2,128)S(1)} %maximum_bitcast_fusion.2), channel_id=4, replica_groups=mesh['ep_0'=8,'ep_1'=4,'ep_2'=2,'tp'=4] {'ep_1'}, dimensions={0}, use_global_device_ids=true | all-gather | bytes 81920 | tf_op jit(solution)/shard_map/all_gather | solution.py:36
  212.0 20.6 %all-gather.7 = f32[8,2,2048]{2,1,0:T(2,128)S(1)} all-gather(f32[1,2,2048]{2,1,0:T(2,128)S(1)} %maximum_bitcast_fusion.3), channel_id=5, replica_groups=mesh['ep_0'=8,'ep_1'=4,'ep_2'=2,'tp'=4] {'ep_0'}, dimensions={0}, use_global_device_ids=true | all-gather | bytes 147456 | tf_op jit(solution)/shard_map/all_gather | solution.py:36
  232.6 3.4 %reshape.839 = bf16[64,5,2048]{2,1,0:T(8,128)(2,1)} reshape(bf16[320,2048]{1,0:T(8,128)(2,1)} %reduce-scatter.2.cloned.1.call-done) | data formatting | bytes 2621440 | tf_op jit(solution)/shard_map/reshape | solution.py:190
  236.1 11.5 %all-to-all-start.1 = ((bf16[64,5,2048]{2,1,0:T(8,128)(2,1)}), bf16[64,5,2048]{2,1,0:T(8,128)(2,1)}, u32[]{:S(2)}, u32[]{:S(2)}) async-start(bf16[64,5,2048]{2,1,0:T(8,128)(2,1)} %reshape.839), calls=%async_computation.2 | async-start | bytes 4194304 | tf_op jit(solution)/shard_map/all_to_all | solution.py:189
  247.9 1.3 fusion.23
  249.2 48.0 %all-to-all-done.1 = bf16[64,5,2048]{2,1,0:T(8,128)(2,1)} async-done(((bf16[64,5,2048]{2,1,0:T(8,128)(2,1)}), bf16[64,5,2048]{2,1,0:T(8,128)(2,1)}, u32[]{:S(2)}, u32[]{:S(2)}) %all-to-all-start.1) | async-done | bytes 1310752 | tf_op jit(solution)/shard_map/all_to_all | solution.py:189
  297.2 2.6 reshape.840
  299.8 1.6 gather_fusion.1
  301.4 0.7 gather.15
  302.2 4.9 %multiply_reduce_fusion = bf16[128,2048]{1,0:T(8,128)(2,1)} fusion(bf16[128,2,2048]{2,1,0:T(2,128)(2,1)S(1)} %gather.15, pred[128,2]{1,0:T(8,128)(4,1)S(1)} %copy-done.7, f32[128,2]{1,0:T(8,128)S(1)} %copy-done.4), kind=kLoop, calls=%fused_computation.14 | loop fusion | flops 1835008 | bytes 1574144 | tf_op jit(solution)/shard_map/reduce_sum | solution.py:199
  (142 shorter events, 10.8 us)
Async XLA Ops:
  7.2 96.8 %copy-start = (bf16[8,256,256]{2,1,0:T(8,128)(2,1)S(1)}, bf16[8,256,256]{2,1,0:T(8,128)(2,1)}, u32[]{:S(2)}) copy-start(bf16[8,256,256]{2,1,0:T(8,128)(2,1)} %param.19) | copy-start | bytes 3145732
  7.2 136.9 %all-gather.10.cloned.1.call-start = ((), (), s32[]{:S(2)}) async-start(), calls=%async_computation.3 | async-start | bytes 6553600 | tf_op jit(solution)/shard_map/all_gather | solution.py:181
  84.6 6.0 %copy-start.9 = (f32[2048]{0:T(1024)S(1)}, f32[2048]{0:T(1024)}, u32[]{:S(2)}) copy-start(f32[2048]{0:T(1024)} %param.21) | copy-start | bytes 24580
  84.6 6.0 %copy-start.8 = (f32[4,2048]{1,0:T(4,128)S(1)}, f32[4,2048]{1,0:T(4,128)}, u32[]{:S(2)}) copy-start(f32[4,2048]{1,0:T(4,128)} %param.18) | copy-start | bytes 98308
  84.6 8.0 %copy-start.10 = (f32[128]{0:T(128)S(1)}, f32[128]{0:T(128)}, u32[]{:S(2)}) copy-start(f32[128]{0:T(128)} %param.22) | copy-start | bytes 1540
  84.6 8.9 %copy-start.11 = (f32[128,2]{0,1:T(2,128)S(1)}, f32[128,2]{0,1:T(2,128)}, u32[]{:S(2)}) copy-start(f32[128,2]{0,1:T(2,128)} %param.25) | copy-start | bytes 3076
  86.1 146.5 %reduce-scatter.2.cloned.1.call-start = ((), (), s32[]{:S(2)}) async-start(), calls=%async_computation.4 | async-start | bytes 6553600 | tf_op jit(solution)/shard_map/reduce_scatter | solution.py:183
  87.2 13.8 %collective-permute-start = (bf16[3,2048]{0,1:T(8,128)(2,1)S(1)}, bf16[3,2048]{0,1:T(8,128)(2,1)S(1)}, u32[]{:S(2)}, u32[]{:S(2)}) collective-permute-start(bf16[3,2048]{0,1:T(8,128)(2,1)S(1)} %copy.55), channel_id=1, source_target_pairs={{0,1},{1,2},{2,3},{3,4},{4,5},{5,6},{6,7},{7,8},{8,9},{9,10},{10,1... | collective-permute-start | bytes 36872 | tf_op jit(solution)/shard_map/ppermute | solution.py:19
  103.1 0.8 copy-start.2
  171.6 0.9 copy-start.5
  171.6 1.0 copy-start.6
  232.6 15.3 %copy-start.3 = (bf16[128,2048]{1,0:T(8,128)(2,1)S(1)}, bf16[128,2048]{1,0:T(8,128)(2,1)}, u32[]{:S(2)}) copy-start(bf16[128,2048]{1,0:T(8,128)(2,1)} %param.16) | copy-start | bytes 1572868
  236.1 61.1 %all-to-all-start.1 = ((bf16[64,5,2048]{2,1,0:T(8,128)(2,1)}), bf16[64,5,2048]{2,1,0:T(8,128)(2,1)}, u32[]{:S(2)}, u32[]{:S(2)}) async-start(bf16[64,5,2048]{2,1,0:T(8,128)(2,1)} %reshape.839), calls=%async_computation.2 | async-start | bytes 4194304 | tf_op jit(solution)/shard_map/all_to_all | solution.py:189
  299.8 2.4 copy-start.4
  299.8 2.4 copy-start.7
  299.8 7.3 %copy-start.1 = (bf16[8,256,256]{2,1,0:T(8,128)(2,1)S(1)}, bf16[8,256,256]{2,1,0:T(8,128)(2,1)}, u32[]{:S(2)}) copy-start(bf16[8,256,256]{2,1,0:T(8,128)(2,1)} %param.19) | copy-start | bytes 3145732
Sparse Core Ops, SparseCore 0:
  86.2 57.8 all-gather.9
  171.7 58.3 reduce-scatter.1
where the time goes:
time: 316 us; the launch traced here: 314 us
  blocking collectives  113 us (36%)
  waiting for transfers between devices  75.8 us (24%)
  local copies, waits for them, and re-layouts  41.1 us (13%)
  matrix products  30.9 us (10%)
  other arithmetic  22.8 us (7%)
  starting transfers between devices  15 us (5%)
  between operations  14.6 us (5%)
    all_to_all x1, blocking collectives, shards(): lax.all_to_all(outgoing, EP, split_axis=0, concat_axis=0, tiled=True)  62.5 us
    all_gather x4, blocking collectives, gathered_once(): both, at, found = (lax.all_gather(jnp.concatenate(lines), axis), 0, {})  50.5 us
    all_to_all x1, waiting for transfers between devices, shards(): lax.all_to_all(route_out.reshape(ep_count, capacity, width_all), EP, spli...  48 us
    all_gather x1, waiting for transfers between devices, shards(): lax.all_gather(arrived.reshape(-1, width_all), 'tp', axis=0, tiled=True)  21 us
    dot_general x1, matrix products, shards(): jnp.dot(hidden, w_down[0], preferred_element_type=jnp.float32)  17.6 us
    all_to_all x1, starting transfers between devices, shards(): lax.all_to_all(route_out.reshape(ep_count, capacity, width_all), EP, spli...  11.5 us
    dot_general x1, matrix products, expert_hidden(): jnp.dot(rows_in, gate_part, preferred_element_type=jnp.float32)  9.94 us
    ppermute x1, waiting for transfers between devices, passed_along(): return lax.ppermute(block, axis, route)  6.82 us
  transfers between devices with their start and end apart: 4, of which 3 were waited for; matrix products, arithmetic and copies ran while one was open for 12% of the time, Pallas kernels for 0%

commit v1 on v0

v1 whole, which is shorter than its diff:
```python
import functools

import jax
import jax.numpy as jnp
from jax import lax
from jax.experimental import pallas as pl
from jax.experimental.pallas import tpu as pltpu
from jax.sharding import Mesh
from jax.sharding import PartitionSpec as P

AXES = ("ep_0", "ep_1", "ep_2", "tp")
EP = ("ep_0", "ep_1", "ep_2")
MESH = pl.DeviceIdType.MESH
EPSILON = 1e-05
CAP = 5
F32 = jnp.float32
BF16 = jnp.bfloat16


def iota(shape, dim):
    return lax.broadcasted_iota(jnp.int32, shape, dim)


def mm(a, b):
    return jnp.dot(a, b, preferred_element_type=F32)


def minus_expm1(x):
    series = 1.0 + x * (1.0 / 7.0)
    for k in (6.0, 5.0, 4.0, 3.0, 2.0):
        series = 1.0 + x * (1.0 / k) * series
    return -jnp.where(x > -0.25, x * series, jnp.exp(x) - 1.0)


def kernel(
    zn, xn, cn, tpn,
    tok, gain, routes, rw, rate, shift, convw,
    rec_h, gate_h, ga_h, gx_h, wg_h, wu_h, wd_h,
    mixed_o, expert_o,
    wgu, wd, ga, gx, rec, gate, halo, hist, dec, sta,
    out, zr, tt, xx, part, ra, rb, rc, cs, rr, rt, rz, ret, hid, whl, acc,
    tot1, tot2, tot3,
    ld, halo_s, halo_r,
    z_s, z_r, x_s, x_r, bx_s, bx_r, bz_s, bz_r,
    y_s, y_r, c1_s, c1_r, c2_s, c2_r, c3_s, c3_r,
):
    xcn = xn * cn
    en = zn * xcn
    z, x, c, tp = (lax.axis_index(name) for name in AXES)
    xc = x * cn + c
    rows, width = tok.shape
    ff = wd.shape[0]
    half = en // 2

    def at_z(k):
        return (lax.rem(z + k, zn), x, c, tp)

    def at_xc(dx, dc):
        return (z, lax.rem(x + dx, xn), lax.rem(c + dc, cn), tp)

    def at_tp(k):
        return (z, x, c, lax.rem(tp + k, tpn))

    def at_xc_abs(k):
        return (z, k // cn, lax.rem(k, cn), tp)

    plus, minus = at_tp(1), at_tp(tpn - 1)
    total = en * tpn
    me = ((z * xn + x) * cn + c) * tpn + tp

    def at_flat(i):
        e = i // tpn
        return (e // xcn, lax.rem(e // cn, xn), lax.rem(e, cn), lax.rem(i, tpn))

    follower, leader = at_flat(lax.rem(me + 1, total)), at_flat(lax.rem(me + total - 1, total))

    def rcopy(src, dst, ss, rs, dev):
        return pltpu.make_async_remote_copy(
            src_ref=src, dst_ref=dst, send_sem=ss, recv_sem=rs, device_id=dev, device_id_type=MESH
        )

    def loop(lo, hi, body):
        def step(i, carry):
            body(i)
            return carry

        lax.fori_loop(lo, hi, step, 0)

    loads = [
        pltpu.make_async_copy(rec_h, rec, ld.at[0]),
        pltpu.make_async_copy(ga_h, ga, ld.at[1]),
        pltpu.make_async_copy(gx_h, gx, ld.at[2]),
        pltpu.make_async_copy(gate_h, gate, ld.at[3]),
        pltpu.make_async_copy(wd_h.at[0], wd, ld.at[4]),
    ]
    for copy in loads:
        copy.start()

    def gu_copy(j, which):
        source = wg_h if which == 0 else wu_h
        return pltpu.make_async_copy(
            source.at[0, :, pl.ds(j * 128, 128)],
            wgu.at[:, pl.ds(j * 256 + which * 128, 128)],
            ld.at[5 + 2 * j + which],
        )

    for j in range(ff // 128):
        gu_copy(j, 0).start()
        gu_copy(j, 1).start()

    barrier = pltpu.get_barrier_semaphore()

    def greet(dev):
        pl.semaphore_signal(barrier, inc=1, device_id=dev, device_id_type=MESH)

    loop(1, zn, lambda k: greet(at_z(k)))
    loop(1, xcn, lambda k: greet(at_xc(k // cn, lax.rem(k, cn))))
    loop(1, tpn, lambda k: greet(at_tp(k)))
    greet(follower)
    greet(leader)

    values = tok[...].astype(F32)
    center = jnp.mean(values, -1, keepdims=True)
    values = values - center
    spread = jnp.mean(jnp.square(values), -1, keepdims=True)
    normed = (values * lax.rsqrt(spread + EPSILON) * gain[...]).astype(BF16)

    eye = iota((rows, rows), 0) == iota((rows, rows), 1)
    before = (iota((rows, rows), 1) < iota((rows, rows), 0)).astype(F32).astype(BF16)
    experts = iota((rows, en), 1)
    picked = [routes[:, k : k + 1] == experts for k in range(2)]
    ones = [p.astype(F32) for p in picked]
    ranks = [mm(before, o.astype(BF16)) for o in ones]
    ranks[1] = ranks[1] + jnp.sum(ones[0], axis=0, keepdims=True)
    place_col, place_row = [], []
    lc, lx = cn.bit_length() - 1, xn.bit_length() - 1
    for k in range(2):
        slot = jnp.sum(ones[k] * ranks[k], axis=1, keepdims=True)
        e = routes[:, k : k + 1]
        dz = ((e >> (lc + lx)) - z) & (zn - 1)
        dx = ((e >> lc) - x) & (xn - 1)
        dc = (e - c) & (cn - 1)
        col = slot * float(en) + (dz * xcn + dx * cn + dc).astype(F32)
        place_col.append(col)
        place_row.append(jnp.sum(jnp.where(eye, col, 0.0), axis=0, keepdims=True))
    pl.semaphore_wait(barrier, zn + xcn + tpn - 3 + 2)

    loads[0].wait()
    halo_copy = rcopy(rec.at[pl.ds(rows - 8, 8)], halo, halo_s.at[0], halo_r.at[0], follower)
    halo_copy.start()

    def z_copy(s, k):
        span = pl.ds(pl.multiple_of(k * xcn, xcn), xcn)
        return rcopy(out.at[s, span], zr.at[s, span], z_s.at[s, k], z_r.at[s, k], at_z(k))

    spots = iota((en, rows), 0).astype(F32)
    for s in range(CAP):
        base = spots + float(s * en)
        take = jnp.where((place_row[0] == base) | (place_row[1] == base), 1.0, 0.0).astype(BF16)
        out[s] = mm(take, normed).astype(BF16)
        loop(1, zn, lambda k, s=s: z_copy(s, k).start())
    lane = iota((rows, 2 * en), 1)
    spot = (lane & (en - 1)).astype(F32)
    for s in range(CAP):
        base = spot + float(s * en)
        weight = jnp.where(place_col[0] == base, rw[:, 0:1], 0.0)
        weight = weight + jnp.where(place_col[1] == base, rw[:, 1:2], 0.0)
        high = weight.astype(BF16).astype(F32)
        whl[s] = jnp.where(lane < en, high, weight - high).astype(BF16)

    shift_col = jnp.sum(jnp.where(eye, shift[...], 0.0), axis=1, keepdims=True)
    loads[1].wait()
    loads[2].wait()
    halo_copy.wait()
    hist[8:, :] = rec[...].astype(F32)
    hist[0:8, :] = jnp.where(me == 0, 0.0, halo[...].astype(F32))
    steps = rows // 8

    def mixer_block(b):
        cols = pl.ds(pl.multiple_of(b * 256, 256), 256)
        conv = jnp.zeros((rows, 256), F32)
        for j in range(4):
            conv = conv + convw[j : j + 1, cols] * hist[5 + j : 5 + j + rows, cols]
        conv = conv.astype(BF16)
        recur = jax.nn.sigmoid(mm(conv, ga[b]))
        enter = jax.nn.sigmoid(mm(conv, gx[b]))
        log_a = shift_col - rate[:, cols] * recur
        decay = jnp.exp(log_a)
        drive = jnp.sqrt(minus_expm1(2.0 * log_a)) * enter * conv.astype(F32)
        for h in range(2):
            n = 2 * b + h
            dec[n] = decay[:, h * 128 : h * 128 + 128]
            sta[n] = drive[:, h * 128 : h * 128 + 128]
            factor, state = dec[n, pl.ds(0, 8, stride=steps)], sta[n, pl.ds(0, 8, stride=steps)]
            for i in range(1, steps):
                at = pl.ds(i, 8, stride=steps)
                a = dec[n, at]
                state = a * state + sta[n, at]
                factor = factor * a
                dec[n, at] = factor
                sta[n, at] = state
            f, t = factor[0:1], state[0:1]
            for g in range(1, 8):
                t = factor[g : g + 1] * t + state[g : g + 1]
                f = factor[g : g + 1] * f
            lanes = pl.ds(pl.multiple_of(n * 128, 128), 128)
            tot1[tp, 0:1, lanes] = f
            tot1[tp, 1:2, lanes] = t

    loop(0, width // 256, mixer_block)

    def t1_copy(k):
        return rcopy(tot1.at[tp], tot1.at[tp], c1_s.at[k], c1_r.at[tp], at_tp(k))

    def t1_wait(k):
        far = lax.rem(tp + k, tpn)
        rcopy(tot1.at[far], tot1.at[far], c1_s.at[k], c1_r.at[far], at_tp(k)).wait_recv()

    def t2_copy(k):
        return rcopy(
            tot2.at[xc], tot2.at[xc], c2_s.at[k], c2_r.at[xc], at_xc_abs(lax.rem(xc + k, xcn))
        )

    def t2_wait(k):
        far = lax.rem(xc + k, xcn)
        rcopy(tot2.at[far], tot2.at[far], c2_s.at[k], c2_r.at[far], at_xc_abs(far)).wait_recv()

    def t3_copy(k):
        return rcopy(tot3.at[z], tot3.at[z], c3_s.at[k], c3_r.at[z], at_z(k))

    def t3_wait(k):
        far = lax.rem(z + k, zn)
        rcopy(tot3.at[far], tot3.at[far], c3_s.at[k], c3_r.at[far], at_z(k)).wait_recv()

    loop(1, tpn, lambda k: t1_copy(k).start())

    def fold(ref, count, here):
        f, t = jnp.ones((1, width), F32), jnp.zeros((1, width), F32)
        fi, ti = f, t
        for k in range(count):
            a, b = ref[k, 0:1, :], ref[k, 1:2, :]
            t = a * t + b
            f = f * a
            inside = k < here
            fi = jnp.where(inside, f, fi)
            ti = jnp.where(inside, t, ti)
        return (f, t), (fi, ti)

    swap_in = iota((en, en), 1) == (iota((en, en), 0) & (zn - 1)) * xcn + (
        iota((en, en), 0) >> (zn.bit_length() - 1)
    )
    swap_in = swap_in.astype(F32).astype(BF16)
    swap_out = iota((en, en), 1) == (iota((en, en), 0) & (xcn - 1)) * zn + (
        iota((en, en), 0) >> (xcn.bit_length() - 1)
    )
    swap_out = swap_out.astype(F32).astype(BF16)

    def x_copy(s, k):
        span = pl.ds(pl.multiple_of(k * zn, zn), zn)
        return rcopy(
            tt.at[s, span], xx.at[s, span], x_s.at[s, k], x_r.at[s, k],
            at_xc(k // cn, lax.rem(k, cn)),
        )

    def bx_copy(s, k):
        span = pl.ds(pl.multiple_of(k * zn, zn), zn)
        return rcopy(
            rr.at[s, span], rt.at[s, span], bx_s.at[s, k], bx_r.at[s, k],
            at_xc(xn - k // cn, cn - lax.rem(k, cn)),
        )

    def bz_copy(s, k):
        span = pl.ds(pl.multiple_of(k * xcn, xcn), xcn)
        return rcopy(rz.at[s, span], ret.at[s, span], bz_s.at[s, k], bz_r.at[s, k], at_z(zn - k))

    def y_copy(s, number):
        def block(b, side):
            return pl.ds(b * en + side * half, half)

        src, dst, dev = {
            0: (xx.at[s, pl.ds(0, en)], xx.at[s, pl.ds(3 * en, en)], plus),
            1: (xx.at[s, pl.ds(0, en)], xx.at[s, pl.ds(en, en)], minus),
            2: (xx.at[s, block(3, 0)], xx.at[s, block(2, 0)], plus),
            3: (xx.at[s, block(1, 1)], xx.at[s, block(2, 1)], minus),
            4: (part.at[s, block(2, 0)], ra.at[s, 0], plus),
            5: (part.at[s, block(2, 1)], ra.at[s, 1], minus),
            6: (part.at[s, block(1, 1)], rb.at[s, 0], plus),
            7: (part.at[s, block(3, 0)], rb.at[s, 1], minus),
            8: (cs.at[s, 0], rc.at[s, 0], plus),
            9: (cs.at[s, 1], rc.at[s, 1], minus),
        }[number]
        return rcopy(src, dst, y_s.at[s, number], y_r.at[s, number], dev)

    def stage0(s):
        loop(1, zn, lambda k: z_copy(s, k).wait_recv())
        zr[s, 0:xcn] = out[s, 0:xcn]
        tt[s] = mm(swap_in, zr[s]).astype(BF16)
        loop(1, xcn, lambda k: x_copy(s, k).start())
        xx[s, 0:zn] = tt[s, 0:zn]

    def stage1(s):
        loop(1, xcn, lambda k: x_copy(s, k).wait_recv())
        y_copy(s, 0).start()
        y_copy(s, 1).start()

    def stage2(s):
        y_copy(s, 0).wait_recv()
        y_copy(s, 2).start()
        y_copy(s, 1).wait_recv()
        y_copy(s, 3).start()

    def stage3(s):
        y_copy(s, 2).wait_recv()
        y_copy(s, 3).wait_recv()

        def up(j):
            pair = mm(xx[s], wgu[:, pl.ds(pl.multiple_of(j * 256, 256), 256)])
            gated, raised = pair[:, :128], pair[:, 128:]
            cols = pl.ds(pl.multiple_of(j * 128, 128), 128)
            hid[:, cols] = (gated * jax.nn.sigmoid(gated) * raised).astype(BF16)

        loop(0, ff // 128, up)

        def down(j):
            cols = pl.ds(pl.multiple_of(j * 256, 256), 256)
            part[s, :, cols] = mm(hid[...], wd[:, cols]).astype(BF16)

        loop(0, width // 256, down)
        for number in (4, 5, 6, 7):
            y_copy(s, number).start()

    def stage4(s):
        for side, b in ((0, 1), (1, 3)):
            y_copy(s, 4 + side).wait_recv()
            mine = part[s, b * en + side * half : b * en + side * half + half]
            cs[s, side] = (ra[s, side].astype(F32) + mine.astype(F32)).astype(BF16)
            y_copy(s, 8 + side).start()

    def stage5(s):
        for number in (6, 7, 8, 9):
            y_copy(s, number).wait_recv()
        for side in range(2):
            mine = part[s, side * half : side * half + half].astype(F32)
            mine = mine + rc[s, side].astype(F32) + rb[s, 1 - side].astype(F32)
            rr[s, side * half : side * half + half] = mine.astype(BF16)
        loop(1, xcn, lambda k: bx_copy(s, k).start())
        rt[s, 0:zn] = rr[s, 0:zn]

    def stage6(s):
        loop(1, xcn, lambda k: bx_copy(s, k).wait_recv())
        rz[s] = mm(swap_out, rt[s]).astype(BF16)
        loop(1, zn, lambda k: bz_copy(s, k).start())
        ret[s, 0:xcn] = rz[s, 0:xcn]

    def stage7(s):
        loop(1, zn, lambda k: bz_copy(s, k).wait_recv())
        back = ret[s]
        acc[...] += mm(whl[s], jnp.concatenate([back, back], 0))

    acc[...] = jnp.zeros_like(acc)
    stages = ((0, stage0), (1, stage1), (2, stage2), (4, stage4), (5, stage5), (6, stage6),
              (7, stage7), (3, stage3))

    def carry_1():
        loop(1, tpn, t1_wait)
        (f, t), _ = fold(tot1, tpn, tp)
        tot2[xc, 0:1, :] = f
        tot2[xc, 1:2, :] = t
        loop(1, xcn, lambda k: t2_copy(k).start())

    def carry_2():
        loop(1, xcn, t2_wait)
        (f, t), _ = fold(tot2, xcn, xc)
        tot3[z, 0:1, :] = f
        tot3[z, 1:2, :] = t
        loop(1, zn, lambda k: t3_copy(k).start())

    def carry_3():
        loop(1, zn, t3_wait)
        _, (_, t3) = fold(tot3, zn, z)
        _, (f2, t2) = fold(tot2, xcn, xc)
        _, (f1, t1) = fold(tot1, tpn, tp)
        hist[0:1, :] = f1 * (f2 * t3 + t2) + t1
        loads[3].wait()

        def finish(n):
            cols = pl.ds(pl.multiple_of(n * 128, 128), 128)
            last = pl.ds(steps - 1, 8, stride=steps)
            factor, state = dec[n, last], sta[n, last]
            starts = [hist[0:1, cols]]
            for g in range(7):
                starts.append(factor[g : g + 1] * starts[-1] + state[g : g + 1])
            start = jnp.concatenate(starts, 0)
            for i in range(steps):
                at = pl.ds(i, 8, stride=steps)
                sta[n, at] = sta[n, at] + dec[n, at] * start
            mixed_o[:, cols] = (
                sta[n] * jax.nn.gelu(gate[:, cols].astype(F32), approximate=True)
            ).astype(BF16)

        loop(0, width // 128, finish)

    def tick(t):
        for number, stage in stages:
            if number == 3:
                @pl.when(t == 3)
                def _():
                    for j in range(ff // 128):
                        gu_copy(j, 0).wait()
                        gu_copy(j, 1).wait()
                    loads[4].wait()

            pl.when((t >= number) & (t < number + CAP))(functools.partial(stage, t - number))
        pl.when(t == 1)(carry_1)
        pl.when(t == 2)(carry_2)
        pl.when(t == 7)(carry_3)

    loop(0, CAP + 7, tick)
    expert_o[...] = acc[...].astype(BF16)

    loop(1, tpn, lambda k: t1_copy(k).wait_send())
    loop(1, xcn, lambda k: t2_copy(k).wait_send())
    loop(1, zn, lambda k: t3_copy(k).wait_send())

    def drain(s):
        loop(1, zn, lambda k: z_copy(s, k).wait_send())
        loop(1, xcn, lambda k: x_copy(s, k).wait_send())
        loop(1, xcn, lambda k: bx_copy(s, k).wait_send())
        loop(1, zn, lambda k: bz_copy(s, k).wait_send())
        for number in range(10):
            y_copy(s, number).wait_send()

    loop(0, CAP, drain)


def shards(
    gate_branch, rec_branch, conv_weight, gate_a, gate_x, decay_param, decay_shift,
    tokens, routes, route_weight, norm_gain, w_gate, w_up, w_down,
):
    zn, xn, cn, tpn = (lax.axis_size(name) for name in AXES)
    en = zn * xn * cn
    rows, width = tokens.shape
    ff = w_gate.shape[2]
    rate = (8.0 * jax.nn.softplus(-decay_param)).reshape(1, width)
    vmem = pl.BlockSpec(memory_space=pltpu.VMEM)
    hbm = pl.BlockSpec(memory_space=pl.ANY)
    dma = pltpu.SemaphoreType.DMA
    scratch = [
        pltpu.VMEM((width, 2 * ff), BF16), pltpu.VMEM((ff, width), BF16),
        pltpu.VMEM(gate_a.shape, BF16), pltpu.VMEM(gate_x.shape, BF16),
        pltpu.VMEM((rows, width), BF16), pltpu.VMEM((rows, width), BF16),
        pltpu.VMEM((8, width), BF16), pltpu.VMEM((rows + 8, width), F32),
        pltpu.VMEM((width // 128, rows, 128), F32), pltpu.VMEM((width // 128, rows, 128), F32),
        pltpu.VMEM((CAP, en, width), BF16), pltpu.VMEM((CAP, en, width), BF16),
        pltpu.VMEM((CAP, en, width), BF16), pltpu.VMEM((CAP, 4 * en, width), BF16),
        pltpu.VMEM((CAP, 4 * en, width), BF16),
        pltpu.VMEM((CAP, 2, en // 2, width), BF16), pltpu.VMEM((CAP, 2, en // 2, width), BF16),
        pltpu.VMEM((CAP, 2, en // 2, width), BF16), pltpu.VMEM((CAP, 2, en // 2, width), BF16),
        pltpu.VMEM((CAP, en, width), BF16), pltpu.VMEM((CAP, en, width), BF16),
        pltpu.VMEM((CAP, en, width), BF16), pltpu.VMEM((CAP, en, width), BF16),
        pltpu.VMEM((4 * en, ff), BF16), pltpu.VMEM((CAP, rows, 2 * en), BF16),
        pltpu.VMEM((rows, width), F32),
        pltpu.VMEM((tpn, 2, width), F32), pltpu.VMEM((xn * cn, 2, width), F32),
        pltpu.VMEM((zn, 2, width), F32),
        dma((5 + 2 * (ff // 128),)), dma((1,)), dma((1,)),
        dma((CAP, zn)), dma((CAP, zn)), dma((CAP, xn * cn)), dma((CAP, xn * cn)),
        dma((CAP, xn * cn)), dma((CAP, xn * cn)), dma((CAP, zn)), dma((CAP, zn)),
        dma((CAP, 10)), dma((CAP, 10)),
        dma((tpn,)), dma((tpn,)), dma((xn * cn,)), dma((xn * cn,)), dma((zn,)), dma((zn,)),
    ]
    shape = jax.ShapeDtypeStruct((rows, width), BF16)
    return pl.pallas_call(
        functools.partial(kernel, zn, xn, cn, tpn),
        out_shape=(shape, shape),
        in_specs=[vmem] * 7 + [hbm] * 7,
        out_specs=(vmem, vmem),
        scratch_shapes=scratch,
        compiler_params=pltpu.CompilerParams(
            collective_id=0, has_side_effects=True, vmem_limit_bytes=64 * 1024 * 1024 - 65536
        ),
    )(
        tokens, norm_gain.reshape(1, width), routes, route_weight, rate,
        decay_shift.reshape(1, rows), conv_weight,
        rec_branch, gate_branch, gate_a, gate_x, w_gate, w_up, w_down,
    )


def solution(mesh):
    shape = (8, 4, 2, mesh.shape["tp"])
    split = Mesh(mesh.devices.reshape(shape), AXES)
    return jax.shard_map(
        shards,
        mesh=split,
        in_specs=(
            P(AXES, None), P(AXES, None), P(), P(), P(), P(), P(AXES),
            P(AXES, None), P(AXES, None), P(AXES, None), P(),
            P(EP, None, "tp"), P(EP, None, "tp"), P(EP, "tp", None),
        ),
        out_specs=(P(AXES, None), P(AXES, None)),
        check_vma=False,
    )
```

time: 316 us -> 148 us (0.47)
  Pallas kernels: 0 us -> 139 us
  blocking collectives: 113 us -> 0 us
  waiting for transfers between devices: 75.8 us -> 0 us
  local copies, waits for them, and re-layouts: 41.1 us -> 6.59 us
  matrix products: 30.9 us -> 0 us
  other arithmetic: 22.8 us -> 1.32 us
  starting transfers between devices: 15 us -> 0 us
  between operations: 14.6 us -> 0.64 us
    pallas_call x0 -> x1, Pallas kernels: none -> 139 us  [shards(): pl.pallas_call(functools.partial(kernel, zn, xn, cn, tpn), out_shape=(sha...]
    all_to_all x1 -> x0, blocking collectives: 62.5 us -> none  [shards(): lax.all_to_all(outgoing, EP, split_axis=0, concat_axis=0, tiled=True)]
    all_gather x4 -> x0, blocking collectives: 50.5 us -> none  [gathered_once(): both, at, found = (lax.all_gather(jnp.concatenate(lines), axis), 0, {})]
    all_to_all x1 -> x0, waiting for transfers between devices: 48 us -> none  [shards(): lax.all_to_all(route_out.reshape(ep_count, capacity, width_all), EP, spli...]
    dot_general x4 -> x0, matrix products: 30.9 us -> none  [the longest x1 17.6 us: shards(): jnp.dot(hidden, w_down[0], preferred_element_type=jnp.float32)]
    all_gather x1 -> x0, waiting for transfers between devices: 21 us -> none  [shards(): lax.all_gather(arrived.reshape(-1, width_all), 'tp', axis=0, tiled=True)]
    all_to_all x1 -> x0, starting transfers between devices: 11.5 us -> none  [shards(): lax.all_to_all(route_out.reshape(ep_count, capacity, width_all), EP, spli...]
    gather x4 -> x0, local copies, waits for them, and re-layouts: 7.73 us -> none  [the longest x2 5.38 us: shards(): outgoing = jnp.take(normed, table, axis=0, mode='fill', fill_value=0)]
  transfers between devices with their start and end apart: 4 -> 0, of which waited for: 3 -> 0; matrix products, arithmetic and copies ran while one was open for 12% -> 0% of each run, Pallas kernels for 0% -> 0%
where the time goes in v1:
time: 148 us
  Pallas kernels  139 us (94%)
  local copies, waits for them, and re-layouts  6.59 us (4%)
    pallas_call x1, Pallas kernels, shards(): pl.pallas_call(functools.partial(kernel, zn, xn, cn, tpn), out_shape=(sha...  139 us
    unnamed x4, local copies, waits for them, and re-layouts  6.59 us

profile of v1, /device:TPU:1, one launch (start us, length us, event | category | flops | bytes accessed | tf_op | source)
XLA Modules:
  0.0 147.5 jit_solution(12813776907032998560)
XLA Ops:
  0.6 1.3 fusion
  1.9 1.4 copy.16.routes
  3.4 1.4 copy.17.rw
  4.8 139.0 %shard_map.149 = (bf16[128,2048]{1,0:T(8,128)(2,1)}, bf16[128,2048]{1,0:T(8,128)(2,1)}) custom-call(bf16[128,2048]{1,0:T(8,128)(2,1)} %tok.1, f32[1,2048]{1,0:T(1,128)} %bitcast.4, s32[128,2]{1,0:T(8,128)} %copy.16.routes, f32[128,2]{1,0:T(8,128)} %copy.17.rw, f32[1,2048]{1,0:T(1,128)} %bitcast.3, f32[1,128]{1,0:T(1,128)} %bitcast.5, f32[4,2048]{1,0:T(4,128)} %convw.1, ...), custom_call_target="tpu_custom_call" | custom-call | tf_op jit(solution)/shard_map/pallas_call | solution.py:472
  143.7 1.9 %copy.20 = bf16[128,2048]{1,0:T(8,128)(2,1)} copy(bf16[128,2048]{1,0:T(8,128)(2,1)} %get-tuple-element.4) | data formatting | bytes 1048576
  145.6 1.9 %copy.21 = bf16[128,2048]{1,0:T(8,128)(2,1)} copy(bf16[128,2048]{1,0:T(8,128)(2,1)} %get-tuple-element.5) | data formatting | bytes 1048576
